TPU v7x, 512 devices: a whole 4x8x8 slice. The times are simulated.
512 devices in a mesh: sp: 32 (over z, x), dp: 16 (over y, core).
Axes of the slice: x: 4, y: 8, z: 8, core: 2. Of those that a mesh axis runs over, the one named last changes fastest.
Arguments:
- normed_input: bfloat16 [10240, 2048], P('sp'), may hold values from -6 to 6
- out_grad: bfloat16 [10240, 2048], P('sp'), may hold values from -6 to 6
- value_weight: bfloat16 [2048, 1024], P(None, 'dp'), may hold values from -0.125 to 0.125
- gate_weight: bfloat16 [2048, 1024], P(None, 'dp'), may hold values from -0.125 to 0.125
- down_weight: bfloat16 [1024, 2048], P('dp'), may hold values from -0.1875 to 0.1875
- conv_kernel: float32 [31, 1024], P(None, 'dp'), may hold values from -5 to 5
- conv_bias: float32 [1024], P('dp'), may hold values from -3 to 3
- norm_gain: float32 [1024], P('dp'), may hold values from 0.1 to 1.9
- norm_shift: float32 [1024], P('dp'), may hold values from -3 to 3
Outputs:
- input_grad: bfloat16 [10240, 2048], P('sp')
- value_grad: float32 [2048, 1024], P('sp', 'dp')
- gate_grad: float32 [2048, 1024], P('sp', 'dp')
- down_grad: float32 [1024, 2048], P('dp', 'sp')
- kernel_grad: float32 [31, 1024], P(None, 'dp')
- bias_grad: float32 [1024], P('dp')
- gain_grad: float32 [1024], P('dp')
- shift_grad: float32 [1024], P('dp')
All inputs are finite; a program needn't handle non-finite values.
Results may differ from a plain program's by a relative error of at most 0.006.
Values may be sent and summed in bfloat16 or wider, within the bound.
A program may use at most 64 MiB of HBM per device.

v0:
```python
import math

import jax
import jax.numpy as jnp
from jax import lax
from jax.sharding import PartitionSpec as P

EPS = 1e-05


def with_halo(block, sides, width):
    for axis, dim in sides:
        count = lax.axis_size(axis)
        forward = [(i, i + 1) for i in range(count - 1)]
        backward = [(target, source) for source, target in forward]
        low = lax.ppermute(
            lax.slice_in_dim(block, block.shape[dim] - width, None, axis=dim), axis, forward
        )
        high = lax.ppermute(lax.slice_in_dim(block, 0, width, axis=dim), axis, backward)
        block = jnp.concatenate([low, block, high], axis=dim)
    return block


def from_everyone(shard, axis):
    copies = jnp.broadcast_to(shard, (lax.axis_size(axis), *shard.shape))
    return lax.all_to_all(copies, axis, split_axis=0, concat_axis=0, tiled=True)


def over_copies(shard, axis):
    everything = from_everyone(shard, axis)
    return jnp.sum(everything, axis=0)


def in_one(arrays, axis):
    ends = [0]
    for a in arrays:
        ends.append(ends[-1] + a.size)
    total = over_copies(jnp.concatenate([a.ravel() for a in arrays]), axis)
    return tuple((total[b:e].reshape(a.shape) for a, b, e in zip(arrays, ends, ends[1:])))


def split_up(shard, dim, count):
    lengths = shard.shape
    tiles = shard.reshape(*lengths[:dim], count, lengths[dim] // count, *lengths[dim + 1 :])
    return jnp.moveaxis(tiles, dim, 0)


def summed_on_arrival(shard, axis, dim):
    count = lax.axis_size(axis)
    tiles = lax.all_to_all(split_up(shard, dim, count), axis, 0, 0, tiled=True)
    return jnp.sum(tiles, axis=0)


def project(weight, rows):
    return lax.dot_general(
        weight, rows, (((0,), (1,)), ((), ())), preferred_element_type=jnp.float32
    )


def on_device(
    normed_input,
    out_grad,
    value_weight,
    gate_weight,
    down_weight,
    conv_kernel,
    conv_bias,
    norm_gain,
    norm_shift,
):
    tokens = normed_input.shape[0]
    width = conv_kernel.shape[0]
    reach = width // 2
    local_channels = value_weight.shape[1]
    channels = local_channels * lax.axis_size("dp")
    ratio = 1.0 / math.sqrt(tokens * lax.axis_size("sp"))
    value_b = project(value_weight, normed_input).astype(jnp.bfloat16)
    gate_b = project(gate_weight, normed_input).astype(jnp.bfloat16)
    value = lax.optimization_barrier(value_b).astype(jnp.float32)
    gate = lax.optimization_barrier(gate_b).astype(jnp.float32)
    opening = jax.nn.sigmoid(gate)
    glu = value * opening
    padded = with_halo(glu, (("sp", 1),), reach)
    mixed = jnp.zeros_like(glu) + conv_bias[:, None]
    for tap in range(width):
        mixed = mixed + conv_kernel[tap][:, None] * padded[:, tap : tap + tokens]
    total, squares = in_one((jnp.sum(mixed, axis=0), jnp.sum(mixed * mixed, axis=0)), "dp")
    mean = total / channels
    spread = squares / channels - mean * mean
    inv_std = lax.rsqrt(spread + EPS)
    centred = (mixed - mean[None, :]) * inv_std[None, :]
    normed = centred * norm_gain[:, None] + norm_shift[:, None]
    sig = jax.nn.sigmoid(normed)
    activated = (normed * sig).astype(jnp.bfloat16)
    d_act = lax.dot_general(
        down_weight, out_grad, (((1,), (1,)), ((), ())), preferred_element_type=jnp.float32
    )
    d_normed = d_act * sig * (1.0 + normed * (1.0 - sig))
    d_centred = d_normed * norm_gain[:, None]
    first, second = in_one((jnp.sum(d_centred, axis=0), jnp.sum(d_centred * centred, axis=0)), "dp")
    d_mixed = inv_std[None, :] * (
        d_centred - first[None, :] / channels - centred * (second[None, :] / channels)
    )
    d_padded = with_halo(d_mixed, (("sp", 1),), reach)
    d_glu = jnp.zeros_like(d_mixed)
    for tap in range(width):
        d_glu = (
            d_glu
            + conv_kernel[tap][:, None] * d_padded[:, 2 * reach - tap : 2 * reach - tap + tokens]
        )
    kernel_local = jnp.stack(
        [jnp.sum(d_mixed * padded[:, tap : tap + tokens], axis=1) for tap in range(width)]
    )
    kernel_grad, bias_grad, gain_grad, shift_grad = in_one(
        (
            kernel_local * ratio,
            jnp.sum(d_mixed, axis=1) * ratio,
            jnp.sum(d_normed * centred, axis=1) * ratio,
            jnp.sum(d_normed, axis=1) * ratio,
        ),
        "sp",
    )
    d_value = (d_glu * opening).astype(jnp.bfloat16)
    d_gate = (d_glu * value * opening * (1.0 - opening)).astype(jnp.bfloat16)
    numbers = (((0,), (1,)), ((), ()))
    value_part = lax.dot_general(normed_input, d_value, numbers, preferred_element_type=jnp.float32)
    gate_part = lax.dot_general(normed_input, d_gate, numbers, preferred_element_type=jnp.float32)
    down_part = lax.dot_general(out_grad, activated, numbers, preferred_element_type=jnp.float32)
    summed = summed_on_arrival(
        jnp.concatenate([value_part, gate_part, down_part], axis=1) * ratio, "sp", 0
    )
    value_grad = summed[:, :local_channels]
    gate_grad = summed[:, local_channels : 2 * local_channels]
    down_grad = summed[:, 2 * local_channels :].T
    numbers = (((0,), (1,)), ((), ()))
    own = lax.dot_general(d_value, value_weight, numbers, preferred_element_type=jnp.float32)
    own = own + lax.dot_general(d_gate, gate_weight, numbers, preferred_element_type=jnp.float32)
    input_grad = lax.psum(own, "dp").astype(jnp.bfloat16)
    return (
        input_grad,
        value_grad,
        gate_grad,
        down_grad,
        kernel_grad,
        bias_grad,
        gain_grad,
        shift_grad,
    )


def solution(mesh):
    in_specs = (
        P("sp", None),
        P("sp", None),
        P(None, "dp"),
        P(None, "dp"),
        P("dp", None),
        P(None, "dp"),
        P("dp"),
        P("dp"),
        P("dp"),
    )
    out_specs = (
        P("sp", None),
        P("sp", "dp"),
        P("sp", "dp"),
        P("dp", "sp"),
        P(None, "dp"),
        P("dp"),
        P("dp"),
        P("dp"),
    )
    return jax.shard_map(
        on_device, mesh=mesh, in_specs=in_specs, out_specs=out_specs, check_vma=False
    )
```

profile of v0, /device:TPU:4, one launch (start us, length us, event | category | flops | bytes accessed | tf_op | source)
XLA Modules:
  0.0 166.0 jit_solution(9701281909924138947)
XLA Ops:
  0.6 0.0 copy-start
  0.6 0.0 copy-start.2
  0.7 1.3 copy-done
  2.0 1.4 convolution_convert_fusion.1
  3.4 0.0 copy-start.5
  3.4 0.0 copy-start.9
  3.4 0.0 copy-start.6
  3.5 0.0 copy-start.10
  3.5 0.5 convolution_convert_fusion
  4.0 0.0 copy-start.11
  4.0 0.1 fusion.130
  4.1 3.1 %collective-permute-start = (f32[64,15]{1,0:T(8,128)S(1)}, f32[64,15]{1,0:T(8,128)S(1)}, u32[]{:S(2)}, u32[]{:S(2)}) collective-permute-start(f32[64,15]{1,0:T(8,128)S(1)} %get-tuple-element.92), channel_id=1, source_target_pairs={{0,16},{16,32},{32,48},{48,64},{64,80},{80,96},{96,112},{112,128},... | collective-permute-start | bytes 11528 | tf_op jit(solution)/shard_map/ppermute | solution.py:16
  7.2 2.7 %collective-permute-start.1 = (f32[64,15]{1,0:T(8,128)S(1)}, f32[64,15]{1,0:T(8,128)S(1)}, u32[]{:S(2)}, u32[]{:S(2)}) collective-permute-start(f32[64,15]{1,0:T(8,128)S(1)} %get-tuple-element.93), channel_id=1, source_target_pairs={{16,0},{32,16},{48,32},{64,48},{80,64},{96,80},{112,96},{128,112},... | collective-permute-start | bytes 11528 | tf_op jit(solution)/shard_map/ppermute | solution.py:19
  10.0 0.0 collective-permute-done
  10.0 3.3 %collective-permute-done.1 = f32[64,15]{1,0:T(8,128)S(1)} collective-permute-done((f32[64,15]{1,0:T(8,128)S(1)}, f32[64,15]{1,0:T(8,128)S(1)}, u32[]{:S(2)}, u32[]{:S(2)}) %collective-permute-start.1) | collective-permute-done | bytes 3872 | tf_op jit(solution)/shard_map/ppermute | solution.py:19
  13.3 1.4 fusion.127
  14.7 0.1 pad_maximum_fusion.4
  14.8 14.7 %all_to_all.23 = f32[16,1,640]{2,1,0:T(1,128)S(1)} all-to-all(f32[16,1,640]{2,1,0:T(1,128)S(1)} %broadcast_in_dim.6), channel_id=1, replica_groups=mesh['sp'=32,'dp'=16] {'dp'}, dimensions={0} | all-to-all | bytes 81920 | tf_op jit(solution)/shard_map/all_to_all | solution.py:26
  29.6 0.1 add_rsqrt_fusion
  29.6 0.0 copy-done.6
  29.6 1.8 %convolution_bitcast_fusion = f32[2048,64]{0,1:T(8,128)S(1)} fusion(bf16[320,2048]{1,0:T(8,128)(2,1)} %param.10, f32[64,320]{1,0:T(8,128)S(1)} %get-tuple-element.89, f32[64]{0:T(128)S(1)} %copy-done.10, f32[64]{0:T(128)S(1)} %copy-done.6, f32[320]{0:T(512)S(1)} %get-tuple-element.134, f32[320]{0:T(512)S(1)} %get-tuple-element.133), kind=kOutput, calls=%fused_computation.1 | convolution fusion | flops 84070400 | bytes 1920000 | tf_op jit(solution)/shard_map/dot_general | solution.py:128
  31.4 2.0 %multiply_reduce_fusion = (f32[64]{0:T(128)S(1)}, f32[320]{0:T(512)S(1)}, f32[320]{0:T(512)S(1)}, f32[64]{0:T(128)S(1)}, f32[64,320]{1,0:T(8,128)S(1)}) fusion(f32[64,320]{1,0:T(8,128)S(1)} %get-tuple-element.89, f32[320]{0:T(512)S(1)} %get-tuple-element.134, f32[320]{0:T(512)S(1)} %get-tuple-element.133, f32[64]{0:T(128)S(1)} %copy-done.6, ...), kind=kOutput, calls=%fused_computation.210 | convolution fusion | flops 84274432 | bytes 1742848 | tf_op jit(solution)/shard_map/dot_general | solution.py:95
  33.4 0.1 pad_maximum_fusion.5
  33.4 0.7 broadcast_in_dim.7
  34.1 3.5 %all-to-all-start.1 = ((f32[16,1,640]{2,1,0:T(1,128)}), f32[16,1,640]{2,1,0:T(1,128)S(1)}, u32[]{:S(2)}, u32[]{:S(2)}) async-start(f32[16,1,640]{2,1,0:T(1,128)} %broadcast_in_dim.7), calls=%async_computation.1 | async-start | bytes 81920 | tf_op jit(solution)/shard_map/all_to_all | solution.py:26
  37.6 0.5 broadcast_multiply_fusion.1
  38.1 0.3 copy.41
  38.5 0.0 copy-start.7
  38.5 0.0 copy-start.8
  38.5 6.8 %all-to-all-done.1 = f32[16,1,640]{2,1,0:T(1,128)S(1)} async-done(((f32[16,1,640]{2,1,0:T(1,128)}), f32[16,1,640]{2,1,0:T(1,128)S(1)}, u32[]{:S(2)}, u32[]{:S(2)}) %all-to-all-start.1) | async-done | bytes 40992 | tf_op jit(solution)/shard_map/all_to_all | solution.py:26
  45.3 0.1 slice_multiply_fusion.1
  45.4 0.6 multiply_reduce_fusion.1
  46.0 0.1 fusion.129
  46.1 0.5 multiply_reduce_fusion.10
  46.6 0.4 multiply_reduce_fusion.26
  47.0 0.6 multiply_reduce_fusion.17
  47.6 0.1 stack.127
  47.7 2.5 %collective-permute-start.2 = (f32[64,15]{1,0:T(8,128)S(1)}, f32[64,15]{1,0:T(8,128)S(1)}, u32[]{:S(2)}, u32[]{:S(2)}) collective-permute-start(f32[64,15]{1,0:T(8,128)S(1)} %get-tuple-element.90), channel_id=1, source_target_pairs={{16,0},{32,16},{48,32},{64,48},{80,64},{96,80},{112,96},{128,112},... | collective-permute-start | bytes 11528 | tf_op jit(solution)/shard_map/ppermute | solution.py:19
  50.2 5.5 %collective-permute-start.3 = (f32[64,15]{1,0:T(8,128)S(1)}, f32[64,15]{1,0:T(8,128)S(1)}, u32[]{:S(2)}, u32[]{:S(2)}) collective-permute-start(f32[64,15]{1,0:T(8,128)S(1)} %get-tuple-element.91), channel_id=1, source_target_pairs={{0,16},{16,32},{32,48},{48,64},{64,80},{80,96},{96,112},{112,128},... | collective-permute-start | bytes 11528 | tf_op jit(solution)/shard_map/ppermute | solution.py:16
  55.7 0.1 mul.869
  55.8 0.0 copy-done.7
  55.8 0.1 concatenate.99
  55.9 0.9 broadcast_in_dim.8
  56.7 16.7 %all-to-all-start.3 = ((f32[32,1,2176]{2,1,0:T(1,128)}), f32[32,1,2176]{2,1,0:T(1,128)}, u32[]{:S(2)}, u32[]{:S(2)}) async-start(f32[32,1,2176]{2,1,0:T(1,128)} %broadcast_in_dim.8), calls=%async_computation.3 | async-start | bytes 557056 | tf_op jit(solution)/shard_map/all_to_all | solution.py:26
  73.5 0.0 collective-permute-done.2
  73.5 0.0 collective-permute-done.3
  73.5 1.4 fusion.3
  74.9 1.2 convolution_bitcast_fusion.2
  76.1 1.2 convolution_bitcast_fusion.1
  77.2 1.4 copy.40
  78.6 2.4 %copy.39 = f32[2048,64]{1,0:T(8,128)} copy(f32[2048,64]{0,1:T(8,128)} %convolution_bitcast_fusion.2) | data formatting | bytes 1048576 | tf_op jit(solution)/shard_map/concatenate | solution.py:130
  81.0 3.2 %maximum_multiply_fusion = f32[32,64,192]{2,1,0:T(8,128)} fusion(f32[32,64,64]{2,1,0:T(8,128)S(1)} %bitcast.117, f32[32,64,64]{2,1,0:T(8,128)S(1)} %bitcast.118, f32[32,64,64]{2,1,0:T(8,128)} %bitcast.119), kind=kLoop, calls=%fused_computation.4 | loop fusion | flops 1179648 | bytes 3145728 | tf_op jit(solution)/shard_map/mul | solution.py:130
  84.2 2.0 %fusion.126 = f32[320,2048]{1,0:T(8,128)} fusion(bf16[2048,64]{0,1:T(8,128)(2,1)S(1)} %copy-done.1, f32[64,320]{1,0:T(8,128)S(1)} %get-tuple-element.88, bf16[64,320]{1,0:T(8,128)(2,1)S(1)} %convolution_convert_fusion), kind=kOutput, calls=%fused_computation.301 | convolution fusion | flops 84008960 | bytes 3006464 | tf_op jit(solution)/shard_map/dot_general | solution.py:136
  86.2 0.0 all-to-all-done.3
  86.2 9.9 %all-to-all-start.2 = ((f32[32,64,192]{2,1,0:T(8,128)}), f32[32,64,192]{2,1,0:T(8,128)S(1)}, u32[]{:S(2)}, u32[]{:S(2)}) async-start(f32[32,64,192]{2,1,0:T(8,128)} %maximum_multiply_fusion), calls=%async_computation.2 | async-start | bytes 4194304 | tf_op jit(solution)/shard_map/all_to_all | solution.py:50
  96.1 3.9 %convolution_add_fusion = f32[320,2048]{1,0:T(8,128)} fusion(f32[320,2048]{1,0:T(8,128)} %fusion.126, bf16[64,320]{1,0:T(8,128)(2,1)S(1)} %copy-done.4, bf16[2048,64]{0,1:T(8,128)(2,1)} %param.12), kind=kOutput, calls=%fused_computation | convolution fusion | flops 84541440 | bytes 5545984 | tf_op jit(solution)/shard_map/dot_general | solution.py:137
  100.0 62.1 %all-reduce.1 = bf16[320,2048]{1,0:T(8,128)(2,1)} all-reduce(f32[320,2048]{1,0:T(8,128)} %convolution_add_fusion), channel_id=1, replica_groups=mesh['sp'=32,'dp'=16] {'dp'}, use_global_device_ids=true, to_apply=%region_6.0 | all-reduce | flops 655360 | bytes 3932160 | tf_op jit(solution)/shard_map/psum | solution.py:138
  162.1 1.1 reduce_sum.419
  163.2 0.7 reshape.87
  163.9 0.6 fusion.131
  164.5 0.0 all-to-all-done.2
  164.5 0.1 reduce_sum.384
  164.6 0.7 slice_bitcast_fusion
  165.3 0.7 copy.38
  (21 shorter events, 0.2 us)
Async XLA Ops:
  0.6 1.3 copy-start
  0.6 2.8 %copy-start.2 = (bf16[2048,64]{0,1:T(8,128)(2,1)S(1)}, bf16[2048,64]{0,1:T(8,128)(2,1)}, u32[]{:S(2)}) copy-start(bf16[2048,64]{0,1:T(8,128)(2,1)} %param.12) | copy-start | bytes 786436
  3.4 6.5 %copy-start.5 = (f32[31,64]{1,0:T(8,128)S(1)}, f32[31,64]{1,0:T(8,128)}, u32[]{:S(2)}) copy-start(f32[31,64]{1,0:T(8,128)} %param.14) | copy-start | bytes 23812
  3.4 9.9 %copy-start.9 = (f32[64]{0:T(128)S(1)}, f32[64]{0:T(128)}, u32[]{:S(2)}) copy-start(f32[64]{0:T(128)} %param.15) | copy-start | bytes 772
  3.4 26.2 %copy-start.6 = (f32[64]{0:T(128)S(1)}, f32[64]{0:T(128)}, u32[]{:S(2)}) copy-start(f32[64]{0:T(128)} %param.16) | copy-start | bytes 772
  3.5 26.2 %copy-start.10 = (f32[64]{0:T(128)S(1)}, f32[64]{0:T(128)}, u32[]{:S(2)}) copy-start(f32[64]{0:T(128)} %param.17) | copy-start | bytes 772
  4.0 27.4 %copy-start.11 = (bf16[64,2048]{1,0:T(8,128)(2,1)S(1)}, bf16[64,2048]{1,0:T(8,128)(2,1)}, u32[]{:S(2)}) copy-start(bf16[64,2048]{1,0:T(8,128)(2,1)} %param.13) | copy-start | bytes 786436
  4.1 5.9 %collective-permute-start = (f32[64,15]{1,0:T(8,128)S(1)}, f32[64,15]{1,0:T(8,128)S(1)}, u32[]{:S(2)}, u32[]{:S(2)}) collective-permute-start(f32[64,15]{1,0:T(8,128)S(1)} %get-tuple-element.92), channel_id=1, source_target_pairs={{0,16},{16,32},{32,48},{48,64},{64,80},{80,96},{96,112},{112,128},... | collective-permute-start | bytes 11528 | tf_op jit(solution)/shard_map/ppermute | solution.py:16
  7.2 6.1 %collective-permute-start.1 = (f32[64,15]{1,0:T(8,128)S(1)}, f32[64,15]{1,0:T(8,128)S(1)}, u32[]{:S(2)}, u32[]{:S(2)}) collective-permute-start(f32[64,15]{1,0:T(8,128)S(1)} %get-tuple-element.93), channel_id=1, source_target_pairs={{16,0},{32,16},{48,32},{64,48},{80,64},{96,80},{112,96},{128,112},... | collective-permute-start | bytes 11528 | tf_op jit(solution)/shard_map/ppermute | solution.py:19
  34.1 11.2 %all-to-all-start.1 = ((f32[16,1,640]{2,1,0:T(1,128)}), f32[16,1,640]{2,1,0:T(1,128)S(1)}, u32[]{:S(2)}, u32[]{:S(2)}) async-start(f32[16,1,640]{2,1,0:T(1,128)} %broadcast_in_dim.7), calls=%async_computation.1 | async-start | bytes 81920 | tf_op jit(solution)/shard_map/all_to_all | solution.py:26
  38.5 17.3 %copy-start.7 = (f32[64]{0:T(128)S(1)}, f32[64]{0:T(128)}, u32[]{:S(2)}) copy-start(f32[64]{0:T(128)} %get-tuple-element.136) | copy-start | bytes 772
  38.5 17.3 %copy-start.8 = (f32[64]{0:T(128)S(1)}, f32[64]{0:T(128)}, u32[]{:S(2)}) copy-start(f32[64]{0:T(128)} %get-tuple-element.137) | copy-start | bytes 772
  47.7 25.7 %collective-permute-start.2 = (f32[64,15]{1,0:T(8,128)S(1)}, f32[64,15]{1,0:T(8,128)S(1)}, u32[]{:S(2)}, u32[]{:S(2)}) collective-permute-start(f32[64,15]{1,0:T(8,128)S(1)} %get-tuple-element.90), channel_id=1, source_target_pairs={{16,0},{32,16},{48,32},{64,48},{80,64},{96,80},{112,96},{128,112},... | collective-permute-start | bytes 11528 | tf_op jit(solution)/shard_map/ppermute | solution.py:19
  50.2 23.3 %collective-permute-start.3 = (f32[64,15]{1,0:T(8,128)S(1)}, f32[64,15]{1,0:T(8,128)S(1)}, u32[]{:S(2)}, u32[]{:S(2)}) collective-permute-start(f32[64,15]{1,0:T(8,128)S(1)} %get-tuple-element.91), channel_id=1, source_target_pairs={{0,16},{16,32},{32,48},{48,64},{64,80},{80,96},{96,112},{112,128},... | collective-permute-start | bytes 11528 | tf_op jit(solution)/shard_map/ppermute | solution.py:16
  56.7 29.5 %all-to-all-start.3 = ((f32[32,1,2176]{2,1,0:T(1,128)}), f32[32,1,2176]{2,1,0:T(1,128)}, u32[]{:S(2)}, u32[]{:S(2)}) async-start(f32[32,1,2176]{2,1,0:T(1,128)} %broadcast_in_dim.8), calls=%async_computation.3 | async-start | bytes 557056 | tf_op jit(solution)/shard_map/all_to_all | solution.py:26
  74.9 1.2 copy-start.3
  81.0 3.2 %copy-start.1 = (bf16[2048,64]{0,1:T(8,128)(2,1)S(1)}, bf16[2048,64]{0,1:T(8,128)(2,1)}, u32[]{:S(2)}) copy-start(bf16[2048,64]{0,1:T(8,128)(2,1)} %param.11) | copy-start | bytes 786436
  86.2 9.9 %copy-start.4 = (bf16[64,320]{1,0:T(8,128)(2,1)S(1)}, bf16[64,320]{1,0:T(8,128)(2,1)}, u32[]{:S(2)}) copy-start(bf16[64,320]{1,0:T(8,128)(2,1)} %copy-done.3) | copy-start | bytes 122884
  86.2 78.3 %all-to-all-start.2 = ((f32[32,64,192]{2,1,0:T(8,128)}), f32[32,64,192]{2,1,0:T(8,128)S(1)}, u32[]{:S(2)}, u32[]{:S(2)}) async-start(f32[32,64,192]{2,1,0:T(8,128)} %maximum_multiply_fusion), calls=%async_computation.2 | async-start | bytes 4194304 | tf_op jit(solution)/shard_map/all_to_all | solution.py:50
where the time goes:
time: 167 us; the launch traced here: 166 us
  blocking collectives  76.8 us (46%)
  starting transfers between devices  43.9 us (26%)
  matrix products  13.9 us (8%)
  other arithmetic  10.3 us (6%)
  waiting for transfers between devices  10.1 us (6%)
  local copies, waits for them, and re-layouts  10 us (6%)
    psum x1, blocking collectives, on_device(): input_grad = lax.psum(own, 'dp').astype(jnp.bfloat16)  62.1 us
    all_to_all x2, starting transfers between devices, from_everyone(): return lax.all_to_all(copies, axis, split_axis=0, concat_axis=0, tiled=True)  20.2 us
    all_to_all x1, blocking collectives, from_everyone(): return lax.all_to_all(copies, axis, split_axis=0, concat_axis=0, tiled=True)  14.7 us
    all_to_all x1, starting transfers between devices, summed_on_arrival(): tiles = lax.all_to_all(split_up(shard, dim, count), axis, 0, 0, tiled=True)  9.91 us
    ppermute x2, starting transfers between devices, with_halo(): lax.ppermute(lax.slice_in_dim(block, block.shape[dim] - width, None, axis...  8.58 us
    all_to_all x2, waiting for transfers between devices, from_everyone(): return lax.all_to_all(copies, axis, split_axis=0, concat_axis=0, tiled=True)  6.81 us
    ppermute x2, starting transfers between devices, with_halo(): lax.ppermute(lax.slice_in_dim(block, 0, width, axis=dim), axis, backward)  5.21 us
    concatenate x3, local copies, waits for them, and re-layouts, on_device(): jnp.concatenate([value_part, gate_part, down_part], axis=1) * ratio  4.05 us
  transfers between devices with their start and end apart: 7, of which 2 were waited for; matrix products, arithmetic and copies ran while one was open for 13% of the time, Pallas kernels for 0%

commit v1 on v0

v1 whole, which is shorter than its diff:
```python
import functools
import math

import jax
import jax.numpy as jnp
from jax import lax
from jax.experimental import pallas as pl
from jax.experimental.pallas import tpu as pltpu
from jax.sharding import PartitionSpec as P

EPS = 1e-05
MESH = pl.DeviceIdType.MESH
X = 4
F32 = jnp.float32
BF16 = jnp.bfloat16
NT = (((1,), (1,)), ((), ()))
NN = (((1,), (0,)), ((), ()))
TN = (((0,), (0,)), ((), ()))
CHUNKS = 4


def dot(a, b, dims):
    return lax.dot_general(a, b, dims, preferred_element_type=F32)


def exact_dot(a, b, dims):
    return lax.dot_general(
        a, b, dims, precision=lax.Precision.HIGHEST, preferred_element_type=F32
    )


def aligned(index, size):
    return pl.ds(pl.multiple_of(index * size, size), size)


def repeat(low, high, body):
    def step(i, carry):
        body(i)
        return carry

    lax.fori_loop(low, high, step, 0)


class RingGather:
    def __init__(self, buf, rows, y, c, count, ring_send, ring_recv, pair_send, pair_recv):
        self.buf, self.rows, self.y, self.c, self.count = buf, rows, y, c, count
        self.ring_send, self.ring_recv = ring_send, ring_recv
        self.pair_send, self.pair_recv = pair_send, pair_recv
        self.half = count // 2

    def copy(self, owner, core, k, target, send, recv):
        ref = self.buf.at[aligned(k, self.rows), aligned(owner * 2 + core, 128)]
        return pltpu.make_async_remote_copy(
            ref, ref, send, recv, device_id={"dp": target}, device_id_type=MESH
        )

    def owner(self, way, h):
        step = -1 - h if way == 0 else 1 + h
        return lax.rem(self.y + step + self.count, self.count)

    def place(self, way, h):
        return self.count - 1 - h if way == 0 else 1 + h

    def takes(self, way, h, part):
        return h < self.half - 1 or (h == self.half - 1 and way == part)

    def ring(self, way, h, k, owner):
        step = 1 if way == 0 else self.count - 1
        target = lax.rem(self.y + step, self.count) * 2 + self.c
        return self.copy(
            owner, self.c, k, target, self.ring_send.at[way, h, k], self.ring_recv.at[way, h, k]
        )

    def pair(self, place, k, owner, core):
        return self.copy(
            owner,
            core,
            k,
            self.y * 2 + 1 - self.c,
            self.pair_send.at[place, k],
            self.pair_recv.at[place, k],
        )

    def start(self, k):
        for way in (0, 1):
            self.ring(way, 0, k, self.y).start()
        self.pair(0, k, self.y, self.c).start()

    def arrive(self, h, k, part):
        for way in (0, 1):
            if self.takes(way, h, part):
                owner = self.owner(way, h)
                self.ring(way, h, k, owner).wait_recv()
                if self.takes(way, h + 1, part):
                    self.ring(way, h + 1, k, owner).start()
                self.pair(self.place(way, h), k, owner, self.c).start()

    def hop(self, h):
        cut = CHUNKS // 2
        repeat(0, cut, lambda k: self.arrive(h, k, 0))
        repeat(cut, CHUNKS, lambda k: self.arrive(h, k, 1))

    def wait_pairs(self, k):
        for place in range(self.count):
            owner = lax.rem(self.y + place, self.count)
            self.pair(place, k, owner, 1 - self.c).wait_recv()

    def drain(self):
        cut = CHUNKS // 2
        for part, low, high in ((0, 0, cut), (1, cut, CHUNKS)):

            def body(k, part=part):
                for way in (0, 1):
                    for h in range(self.half):
                        if self.takes(way, h, part):
                            self.ring(way, h, k, self.y).wait_send()
                for place in range(self.count):
                    self.pair(place, k, self.y, self.c).wait_send()

            repeat(low, high, body)


def kernel(
    n_sp,
    n_dp,
    x_hbm,
    og_hbm,
    wv_hbm,
    wg_hbm,
    dw_hbm,
    ck_ref,
    cb_ref,
    ng_ref,
    ns_ref,
    ig_hbm,
    vg_out,
    dg_out,
    kg_out,
    x_ref,
    og_ref,
    wv_ref,
    wg_ref,
    dw_ref,
    w_ref,
    wall_ref,
    vg_ref,
    glu_ref,
    open_ref,
    dact_ref,
    mix_ref,
    cen_ref,
    inv_ref,
    dn_ref,
    dc_ref,
    act_ref,
    dm_ref,
    dvg_ref,
    g_ref,
    out_ref,
    stat_ref,
    pd_ref,
    pv_ref,
    rd_ref,
    rv_ref,
    s_ref,
    own_ref,
    rz_ref,
    kx_ref,
    kz_ref,
    load_sem,
    halo_send,
    halo_recv,
    wsend,
    wrecv,
    ssend,
    srecv,
    ring_send,
    ring_recv,
    pair_send,
    pair_recv,
    xsend,
    xrecv,
    zsend,
    zrecv,
    store_sem,
):
    T, D = x_ref.shape
    CL = cb_ref.shape[-1]
    KW = ck_ref.shape[0]
    C = CL * n_dp
    Z = n_sp // X
    Y = n_dp // 2
    PR = D // n_sp
    ratio = 1.0 / math.sqrt(T * n_sp)
    sp, dp = lax.axis_index("sp"), lax.axis_index("dp")
    z, x = sp // X, lax.rem(sp, X)
    y, c = dp // 2, lax.rem(dp, 2)

    loads = [
        pltpu.make_async_copy(a, b, load_sem.at[i])
        for i, (a, b) in enumerate(
            (
                (wv_hbm, wv_ref),
                (wg_hbm, wg_ref),
                (x_hbm, x_ref),
                (og_hbm, og_ref),
                (dw_hbm, dw_ref),
            )
        )
    ]
    for load in loads:
        load.start()

    def peer_dp(off):
        return lax.rem(dp + off, n_dp)

    def peer_x(off):
        return z * X + lax.rem(x + off, X)

    def peer_z(off):
        return lax.rem(z + off, Z) * X + x

    barrier = pltpu.get_barrier_semaphore()
    for off in range(1, n_dp):
        pl.semaphore_signal(barrier, 1, device_id={"dp": peer_dp(off)}, device_id_type=MESH)
    for off in range(1, X):
        pl.semaphore_signal(barrier, 1, device_id={"sp": peer_x(off)}, device_id_type=MESH)
    for off in range(1, Z):
        pl.semaphore_signal(barrier, 1, device_id={"sp": peer_z(off)}, device_id_type=MESH)

    @pl.when(sp > 0)
    def _():
        pl.semaphore_signal(barrier, 1, device_id={"sp": sp - 1}, device_id_type=MESH)

    @pl.when(sp < n_sp - 1)
    def _():
        pl.semaphore_signal(barrier, 1, device_id={"sp": sp + 1}, device_id_type=MESH)

    loads[0].wait()
    loads[1].wait()
    w_ref[...] = jnp.concatenate([wv_ref[...], wg_ref[...]], axis=1)
    wall_ref[:, aligned(dp, 128)] = w_ref[aligned(dp, 128), :]
    loads[2].wait()
    vg_ref[32 : 32 + T, :] = dot(x_ref[...], w_ref[...], NN).astype(BF16)

    ends = jnp.where(sp > 0, 1, 0) + jnp.where(sp < n_sp - 1, 1, 0)
    pl.semaphore_wait(barrier, n_dp - 1 + X - 1 + Z - 1 + ends)

    def halo(ref, way, height, base, i):
        if way == 0:
            src, dst, target = base + T - height, base - height, sp + 1
        else:
            src, dst, target = base, base + T, sp - 1
        return pltpu.make_async_remote_copy(
            ref.at[pl.ds(src, height), :],
            ref.at[pl.ds(dst, height), :],
            halo_send.at[i, way],
            halo_recv.at[i, way],
            device_id={"sp": target},
            device_id_type=MESH,
        )

    def vg_halo(way):
        return halo(vg_ref, way, 32, 32, 0)

    def dact_halo(way):
        return halo(dact_ref, way, 16, 16, 1)

    @pl.when(sp < n_sp - 1)
    def _():
        vg_halo(0).start()

    @pl.when(sp > 0)
    def _():
        vg_halo(1).start()

    @pl.when(sp == 0)
    def _():
        vg_ref[0:32, :] = jnp.zeros((32, 2 * CL), BF16)
        dact_ref[0:16, :] = jnp.zeros((16, 2 * CL), F32)

    @pl.when(sp == n_sp - 1)
    def _():
        vg_ref[32 + T : 64 + T, :] = jnp.zeros((32, 2 * CL), BF16)
        dact_ref[16 + T : 32 + T, :] = jnp.zeros((16, 2 * CL), F32)

    def weights(off):
        target = peer_dp(off)
        return pltpu.make_async_remote_copy(
            w_ref.at[aligned(target, 128), :],
            wall_ref.at[:, aligned(dp, 128)],
            wsend.at[off],
            wrecv.at[off],
            device_id={"dp": target},
            device_id_type=MESH,
        )

    far = sorted(range(1, n_dp), key=lambda off: -min(off, n_dp - off))
    first_batch = [o for o in far if min(o, n_dp - o) in (5, 6, 7)]
    second_batch = [o for o in far if min(o, n_dp - o) in (8, 1)]
    third_batch = [o for o in far if min(o, n_dp - o) in (2, 3, 4)]
    for off in first_batch:
        weights(off).start()

    loads[3].wait()
    loads[4].wait()
    d_act = dot(og_ref[...], dw_ref[...], NT)
    dact_ref[16 : 16 + T, :] = jnp.concatenate([d_act, jnp.zeros_like(d_act)], axis=1)

    @pl.when(sp < n_sp - 1)
    def _():
        dact_halo(0).start()

    @pl.when(sp > 0)
    def _():
        dact_halo(1).start()

    E = T + 32
    EP = -(-E // 128) * 128
    mix_ref[E:EP, :] = jnp.zeros((EP - E, CL), F32)
    dact_ref[E:EP, :] = jnp.zeros((EP - E, 2 * CL), F32)

    @pl.when(sp > 0)
    def _():
        vg_halo(0).wait_recv()

    @pl.when(sp < n_sp - 1)
    def _():
        vg_halo(1).wait_recv()

    def gate_block(i):
        rows = aligned(i, 64)
        both = vg_ref[rows, :].astype(F32)
        opening = jax.nn.sigmoid(both[:, CL:])
        open_ref[rows, :] = opening
        glu_ref[rows, :] = both[:, :CL] * opening

    repeat(0, (T + 64) // 64, gate_block)

    def conv_block(i):
        acc = jnp.broadcast_to(cb_ref[...], (32, CL))
        for k in range(KW):
            acc = acc + ck_ref[k : k + 1, :] * glu_ref[pl.ds(i * 32 + k + 1, 32), :]
        mix_ref[aligned(i, 32), :] = acc

    repeat(0, E // 32, conv_block)

    n_blocks = EP // 128
    row8 = lax.broadcasted_iota(jnp.int32, (8, CL), 0)

    def pick(j):
        return jnp.where(row8 == j, 1.0, 0.0).astype(F32)

    def packed(first, second):
        total = None
        for j in range(n_blocks):
            term = exact_dot(pick(j), first(j), NT) + exact_dot(pick(n_blocks + j), second(j), NT)
            total = term if total is None else total + term
        return total

    def rows_of(j):
        return pl.ds(j * 128, 128)

    def stat(phase, off):
        return pltpu.make_async_remote_copy(
            stat_ref.at[phase, dp],
            stat_ref.at[phase, dp],
            ssend.at[phase, off],
            srecv.at[phase, off],
            device_id={"dp": peer_dp(off)},
            device_id_type=MESH,
        )

    def stat_arrived(phase, off):
        src = lax.rem(dp + n_dp - off, n_dp)
        pltpu.make_async_remote_copy(
            stat_ref.at[phase, src],
            stat_ref.at[phase, src],
            ssend.at[phase, off],
            srecv.at[phase, off],
            device_id={"dp": peer_dp(off)},
            device_id_type=MESH,
        ).wait_recv()

    def summed(phase):
        for off in far:
            stat_arrived(phase, off)
        return jnp.sum(stat_ref[phase], axis=0)

    def spread_out(table, j):
        return exact_dot(jnp.transpose(table), pick(j), NN)

    stat_ref[0, dp] = packed(
        lambda j: mix_ref[rows_of(j), :], lambda j: mix_ref[rows_of(j), :] * mix_ref[rows_of(j), :]
    )
    for off in far:
        stat(0, off).start()
    for off in second_batch:
        weights(off).start()

    @pl.when(sp > 0)
    def _():
        dact_halo(0).wait_recv()

    @pl.when(sp < n_sp - 1)
    def _():
        dact_halo(1).wait_recv()

    totals = summed(0) * (1.0 / C)
    mean8 = totals
    power8 = pltpu.roll(totals, 8 - n_blocks, 0)
    inv8 = lax.rsqrt(jnp.maximum(power8 - mean8 * mean8, 0.0) + EPS)
    gain = ng_ref[...]
    shift = ns_ref[...]
    for j in range(n_blocks):
        rows = rows_of(j)
        mean = spread_out(mean8, j)
        inv = spread_out(inv8, j)
        cen = (mix_ref[rows, :] - mean) * inv
        normed = cen * gain + shift
        sig = jax.nn.sigmoid(normed)
        dn = dact_ref[rows, 0:CL] * sig * (1.0 + normed * (1.0 - sig))
        inv_ref[rows, :] = inv
        cen_ref[rows, :] = cen
        act_ref[rows, :] = (normed * sig).astype(BF16)
        dn_ref[rows, :] = dn
        dc_ref[rows, :] = dn * gain
    stat_ref[1, dp] = packed(
        lambda j: dc_ref[rows_of(j), :], lambda j: dc_ref[rows_of(j), :] * cen_ref[rows_of(j), :]
    )
    for off in far:
        stat(1, off).start()
    for off in third_batch:
        weights(off).start()

    def x_copy(src, dst, kind, off):
        return pltpu.make_async_remote_copy(
            src,
            dst,
            xsend.at[kind, off],
            xrecv.at[kind, off],
            device_id={"sp": peer_x(off)},
            device_id_type=MESH,
        )

    def x_part(kind, off):
        src, dst = ((pd_ref, rd_ref), (pv_ref, rv_ref))[kind]
        return x_copy(src.at[lax.rem(x + off, X)], dst.at[off - 1], kind, off)

    wide = D // Z
    fold = PR // 2
    act_own = act_ref[16 : 16 + T, :]

    def down_part(i):
        part = dot(og_ref[:, aligned(i, wide)], act_own, TN).astype(BF16)
        for q in range(X):
            piece = part[q * PR : (q + 1) * PR, :]
            pd_ref[q, i] = jnp.concatenate([piece[:fold], piece[fold:]], axis=1)

    repeat(0, Z, down_part)
    for off in (2, 1, 3):
        x_part(0, off).start()

    totals = summed(1) * (1.0 / C)
    second8 = pltpu.roll(totals, 8 - n_blocks, 0)
    for j in range(n_blocks):
        rows = rows_of(j)
        dm = inv_ref[rows, :] * (
            dc_ref[rows, :] - spread_out(totals, j) - cen_ref[rows, :] * spread_out(second8, j)
        )
        token = sp * T - 16 + j * 128 + lax.broadcasted_iota(jnp.int32, (128, CL), 0)
        dm_ref[rows, :] = jnp.where((token >= 0) & (token < n_sp * T), dm, 0.0)

    def back_block(i):
        acc = jnp.zeros((32, CL), F32)
        for k in range(KW):
            acc = acc + ck_ref[k : k + 1, :] * dm_ref[pl.ds(i * 32 + KW - k, 32), :]
        rows = pl.ds(pl.multiple_of(i * 32 + 32, 32), 32)
        opening = open_ref[rows, :]
        value = vg_ref[rows, 0:CL].astype(F32)
        both = jnp.concatenate([acc * opening, acc * value * opening * (1.0 - opening)], axis=1)
        dvg_ref[aligned(i, 32), :] = both.astype(BF16)

    repeat(0, T // 32, back_block)
    g_ref[:, aligned(dp, 128)] = dvg_ref[...]

    tall = T // CHUNKS
    gather_d = RingGather(
        g_ref, tall, y, c, Y, ring_send.at[0], ring_recv.at[0], pair_send.at[0], pair_recv.at[0]
    )
    gather_o = RingGather(
        out_ref, tall, y, c, Y, ring_send.at[1], ring_recv.at[1], pair_send.at[1], pair_recv.at[1]
    )
    repeat(0, CHUNKS, gather_d.start)

    d_own = dvg_ref[...]

    def value_part(i):
        part = dot(x_ref[:, aligned(i, wide)], d_own, TN).astype(BF16)
        pv_ref[:, i] = part.reshape(X, PR, 2 * CL)

    repeat(0, Z, value_part)
    for off in (2, 1, 3):
        x_part(1, off).start()

    def tap_block(i, taps):
        d = dm_ref[pl.ds(pl.multiple_of(i * 8 + 16, 8), 8), :]
        return tuple(
            t + d * glu_ref[pl.ds(i * 8 + k + 17, 8), :] for k, t in enumerate(taps)
        )

    taps = lax.fori_loop(
        0, T // 8, tap_block, tuple(jnp.zeros((8, CL), F32) for _ in range(KW))
    )
    sums = [jnp.sum(t, axis=0, keepdims=True) for t in taps]
    sums.append(jnp.sum(dm_ref[16 : 16 + T, :], axis=0, keepdims=True))
    sums.append(
        jnp.sum(dn_ref[16 : 16 + T, :] * cen_ref[16 : 16 + T, :], axis=0, keepdims=True)
    )
    sums.append(jnp.sum(dn_ref[16 : 16 + T, :], axis=0, keepdims=True))
    sums.append(jnp.zeros((48 - KW - 3, CL), F32))
    table = jnp.concatenate(sums, axis=0)
    kx_ref[x] = jnp.concatenate([table[:24], table[24:]], axis=1)

    def kx_copy(off):
        return x_copy(kx_ref.at[x], kx_ref.at[x], 2, off)

    for off in (2, 1, 3):
        kx_copy(off).start()

    for h in range(Y // 2):
        gather_d.hop(h)

    for off in far:
        weights(off).wait_recv()

    def product(k):
        gather_d.wait_pairs(k)
        rows = aligned(k, tall)
        out = dot(g_ref[rows, :], wall_ref[...], NT)
        out_ref[rows, aligned(dp, 128)] = out.astype(BF16)
        gather_o.start(k)

    repeat(0, CHUNKS, product)

    def kx_arrived(off):
        src = lax.rem(x + X - off, X)
        return x_copy(kx_ref.at[src], kx_ref.at[src], 2, off)

    for off in (1, 3, 2):
        x_part(0, off).wait_recv()
        x_part(1, off).wait_recv()
        kx_arrived(off).wait_recv()

    def x_sum(i):
        d = pd_ref[x, i].astype(F32)
        v = pv_ref[x, i].astype(F32)
        for slot in range(X - 1):
            d = d + rd_ref[slot, i].astype(F32)
            v = v + rv_ref[slot, i].astype(F32)
        s_ref[i, 0:PR] = v.astype(BF16)
        s_ref[i, PR : PR + fold] = d.astype(BF16)

        @pl.when(i == z)
        def _():
            own_ref[0:PR] = v
            own_ref[PR : PR + fold] = d

    repeat(0, Z, x_sum)
    kz_ref[z] = (kx_ref[0] + kx_ref[1]) + (kx_ref[2] + kx_ref[3])

    def z_copy(src, dst, kind, off):
        return pltpu.make_async_remote_copy(
            src,
            dst,
            zsend.at[kind, off],
            zrecv.at[kind, off],
            device_id={"sp": peer_z(off)},
            device_id_type=MESH,
        )

    def z_part(off):
        return z_copy(s_ref.at[lax.rem(z + off, Z)], rz_ref.at[off - 1], 0, off)

    def kz_copy(off):
        return z_copy(kz_ref.at[z], kz_ref.at[z], 1, off)

    z_far = sorted(range(1, Z), key=lambda off: -min(off, Z - off))
    for off in z_far:
        z_part(off).start()
    for off in z_far:
        kz_copy(off).start()

    for h in range(Y // 2):
        gather_o.hop(h)

    def store(k):
        rows = aligned(k, tall)
        return pltpu.make_async_copy(out_ref.at[rows, :], ig_hbm.at[rows, :], store_sem.at[k])

    def finish(k):
        gather_o.wait_pairs(k)
        store(k).start()

    repeat(0, CHUNKS, finish)

    for off in z_far:
        z_part(off).wait_recv()
    total = own_ref[...]
    for off in range(1, Z):
        total = total + rz_ref[off - 1].astype(F32)
    total = total * ratio
    vg_out[...] = total[0:PR]
    dg_out[...] = total[PR : PR + fold]

    for off in z_far:
        src = lax.rem(z + Z - off, Z)
        z_copy(kz_ref.at[src], kz_ref.at[src], 1, off).wait_recv()
    k_total = kz_ref[0]
    for i in range(1, Z):
        k_total = k_total + kz_ref[i]
    kg_out[...] = k_total * ratio

    @pl.when(sp < n_sp - 1)
    def _():
        vg_halo(0).wait_send()
        dact_halo(0).wait_send()

    @pl.when(sp > 0)
    def _():
        vg_halo(1).wait_send()
        dact_halo(1).wait_send()

    for off in far:
        weights(off).wait_send()
        stat(0, off).wait_send()
        stat(1, off).wait_send()
    for off in range(1, X):
        x_part(0, off).wait_send()
        x_part(1, off).wait_send()
        kx_copy(off).wait_send()
    for off in z_far:
        z_part(off).wait_send()
        kz_copy(off).wait_send()
    gather_d.drain()
    gather_o.drain()
    repeat(0, CHUNKS, lambda k: store(k).wait())


def run(n_sp, n_dp, *args):
    x, og, wv, wg, dw, ck, cb, ng, ns = args
    T, D = x.shape
    CL = wv.shape[1]
    Z, Y = n_sp // X, n_dp // 2
    PR = D // n_sp
    E = T + 32
    EP = -(-E // 128) * 128
    vmem = pl.BlockSpec(memory_space=pltpu.VMEM)
    hbm = pl.BlockSpec(memory_space=pl.ANY)
    dma = pltpu.SemaphoreType.DMA
    half = Y // 2
    V = pltpu.VMEM
    outs = pl.pallas_call(
        functools.partial(kernel, n_sp, n_dp),
        out_shape=(
            jax.ShapeDtypeStruct((T, D), BF16),
            jax.ShapeDtypeStruct((PR, 2 * CL), F32),
            jax.ShapeDtypeStruct((PR // 2, 2 * CL), F32),
            jax.ShapeDtypeStruct((24, 2 * CL), F32),
        ),
        in_specs=[hbm] * 5 + [vmem] * 4,
        out_specs=(hbm, vmem, vmem, vmem),
        scratch_shapes=[
            V((T, D), BF16),
            V((T, D), BF16),
            V((D, CL), BF16),
            V((D, CL), BF16),
            V((CL, D), BF16),
            V((D, 2 * CL), BF16),
            V((128, n_dp * 128), BF16),
            V((T + 64, 2 * CL), BF16),
            V((T + 64, CL), F32),
            V((T + 64, CL), F32),
            V((EP, 2 * CL), F32),
            V((EP, CL), F32),
            V((EP, CL), F32),
            V((EP, CL), F32),
            V((EP, CL), F32),
            V((EP, CL), F32),
            V((EP, CL), BF16),
            V((EP, CL), F32),
            V((T, 2 * CL), BF16),
            V((T, n_dp * 128), BF16),
            V((T, D), BF16),
            V((2, n_dp, 8, 128), F32),
            V((X, Z, PR // 2, 2 * CL), BF16),
            V((X, Z, PR, 2 * CL), BF16),
            V((X - 1, Z, PR // 2, 2 * CL), BF16),
            V((X - 1, Z, PR, 2 * CL), BF16),
            V((Z, PR + PR // 2, 2 * CL), BF16),
            V((PR + PR // 2, 2 * CL), F32),
            V((Z - 1, PR + PR // 2, 2 * CL), BF16),
            V((X, 24, 2 * CL), F32),
            V((Z, 24, 2 * CL), F32),
            dma((5,)),
            dma((2, 2)),
            dma((2, 2)),
            dma((n_dp,)),
            dma((n_dp,)),
            dma((2, n_dp)),
            dma((2, n_dp)),
            dma((2, 2, half, CHUNKS)),
            dma((2, 2, half, CHUNKS)),
            dma((2, Y, CHUNKS)),
            dma((2, Y, CHUNKS)),
            dma((3, X)),
            dma((3, X)),
            dma((2, Z)),
            dma((2, Z)),
            dma((CHUNKS,)),
        ],
        compiler_params=pltpu.CompilerParams(collective_id=0, has_side_effects=True),
    )(x, og, wv, wg, dw, ck, cb[None, :], ng[None, :], ns[None, :])
    ig, vg, dg, kg = outs
    KW = ck.shape[0]
    down = jnp.concatenate([dg[:, :CL], dg[:, CL:]], axis=0).T
    table = jnp.concatenate([kg[:, :CL], kg[:, CL:]], axis=0)
    return (
        ig,
        vg[:, :CL],
        vg[:, CL:],
        down,
        table[:KW],
        table[KW],
        table[KW + 1],
        table[KW + 2],
    )


def solution(mesh):
    n_sp, n_dp = mesh.shape["sp"], mesh.shape["dp"]
    in_specs = (
        P("sp", None),
        P("sp", None),
        P(None, "dp"),
        P(None, "dp"),
        P("dp", None),
        P(None, "dp"),
        P("dp"),
        P("dp"),
        P("dp"),
    )
    out_specs = (
        P("sp", None),
        P("sp", "dp"),
        P("sp", "dp"),
        P("dp", "sp"),
        P(None, "dp"),
        P("dp"),
        P("dp"),
        P("dp"),
    )
    return jax.shard_map(
        functools.partial(run, n_sp, n_dp),
        mesh=mesh,
        in_specs=in_specs,
        out_specs=out_specs,
        check_vma=False,
    )
```

time: 167 us -> 81.3 us (0.49)
  the two profiles are of different devices: /device:TPU:4 before, /device:TPU:1 now
where the time goes in v1:
time: 81.3 us; the launch traced here: 80.8 us
  Pallas kernels  67.8 us (83%)
  local copies, waits for them, and re-layouts  11.7 us (14%)
    pallas_call x1, Pallas kernels, run(): pl.pallas_call(functools.partial(kernel, n_sp, n_dp), out_shape=(jax.Shap...  67.8 us
    unnamed x4, local copies, waits for them, and re-layouts  7.15 us

profile of v1, /device:TPU:1, one launch (start us, length us, event | category | flops | bytes accessed | tf_op | source)
XLA Modules:
  0.0 80.8 jit_solution(9187108348466089026)
XLA Ops:
  0.6 2.0 %copy.17.wv_hbm = bf16[2048,64]{1,0:T(8,128)(2,1)} copy(bf16[2048,64]{0,1:T(8,128)(2,1)} %param.11) | data formatting | bytes 524288 | tf_op args[2]
  2.6 2.0 %copy.18.wg_hbm = bf16[2048,64]{1,0:T(8,128)(2,1)} copy(bf16[2048,64]{0,1:T(8,128)(2,1)} %param.12) | data formatting | bytes 524288 | tf_op args[3]
  4.6 67.8 %shard_map.152 = (bf16[320,2048]{1,0:T(8,128)(2,1)}, f32[64,128]{1,0:T(8,128)}, f32[32,128]{1,0:T(8,128)}, f32[24,128]{1,0:T(8,128)}) custom-call(bf16[320,2048]{1,0:T(8,128)(2,1)} %x_hbm.1, bf16[320,2048]{1,0:T(8,128)(2,1)} %og_hbm.1, bf16[2048,64]{1,0:T(8,128)(2,1)} %copy.17.wv_hbm, bf16[2048,64]{1,0:T(8,128)(2,1)} %copy.18.wg_hbm, ...), custom_call_target="tpu_custom_call" | custom-call | tf_op jit(solution)/shard_map/pallas_call | solution.py:663
  72.4 1.3 %slice_bitcast_fusion = (f32[64]{0:T(128)}, f32[64]{0:T(128)}, f32[64]{0:T(128)}) fusion(f32[24,128]{1,0:T(8,128)} %get-tuple-element.15), kind=kLoop, calls=%fused_computation.2 | loop fusion | bytes 1536 | tf_op jit(solution)/shard_map/squeeze | solution.py:736
  73.8 0.9 %fusion.2 = (f32[24,64]{1,0:T(8,128)S(1)}, f32[24,64]{1,0:T(8,128)S(1)}) fusion(f32[24,128]{1,0:T(8,128)} %get-tuple-element.15), kind=kLoop, calls=%fused_computation.7 | loop fusion | bytes 24576 | tf_op jit(solution)/shard_map/slice | solution.py:727
  74.6 0.6 pad_maximum_fusion
  75.2 0.9 %fusion.1 = (f32[32,64]{1,0:T(8,128)S(1)}, f32[32,64]{1,0:T(8,128)S(1)}) fusion(f32[32,128]{1,0:T(8,128)} %get-tuple-element.14), kind=kLoop, calls=%fused_computation.6 | loop fusion | bytes 32768 | tf_op jit(solution)/shard_map/slice | solution.py:726
  76.1 0.7 copy.19
  76.8 1.5 %fusion = (f32[64,64]{1,0:T(8,128)}, f32[64,64]{1,0:T(8,128)}) fusion(f32[64,128]{1,0:T(8,128)} %get-tuple-element.13), kind=kLoop, calls=%fused_computation.5 | loop fusion | bytes 65536 | tf_op jit(solution)/shard_map/slice | solution.py:731
  78.3 2.5 %copy.21 = bf16[320,2048]{1,0:T(8,128)(2,1)} copy(bf16[320,2048]{1,0:T(8,128)(2,1)} %get-tuple-element.41) | data formatting | bytes 2621440
  (1 shorter events, 0.0 us)
